TPU v7x, 32 devices: a whole 2x2x4 slice. The times are simulated.
32 devices in a mesh: fs: 16 (over z, y, x), tp: 2 (over core).
Axes of the slice: x: 2, y: 2, z: 4, core: 2. Of those that a mesh axis runs over, the one named last changes fastest.
Arguments:
- tokens: bfloat16 [6144, 2048], P('fs', 'tp'), may hold values from -24 to 24, as said below
- mixer_gain: float32 [2048], replicated, may hold values from 0.1 to 1.9
- w_content: float32 [2048, 1024], P('fs', 'tp'), may hold values from -0.125 to 0.125
- w_spatial: float32 [2048, 1024], P('fs', 'tp'), may hold values from -0.125 to 0.125
- content_scale: float32 [1024], P('tp'), may hold values from 0.5 to 2
- spatial_scale: float32 [1024], P('tp'), may hold values from 0.2 to 3.5, as said below
- spatial_gain: float32 [1024], P('tp'), may hold values from 0.1 to 1.9
- block_mixing: bfloat16 [8, 128, 128], P('tp'), may hold values from -0.5 to 0.5
- block_bias: float32 [8, 128], P('tp'), may hold values from -6 to 6
- w_project: float32 [1024, 2048], P('tp', 'fs'), may hold values from -0.1875 to 0.1875
- project_scale: float32 [2048], P('fs'), may hold values from 0.5 to 2
- channel_gain: float32 [2048], replicated, may hold values from 0.1 to 1.9
- w_up: float32 [2048, 8192], P('fs', 'tp'), may hold values from -0.125 to 0.125
- up_scale: float32 [8192], P('tp'), may hold values from 0.5 to 2
- w_down: float32 [8192, 2048], P('tp', 'fs'), may hold values from -0.0625 to 0.0625
- down_scale: float32 [2048], P('fs'), may hold values from 0.5 to 2
Outputs:
- layer_out: bfloat16 [6144, 2048], P('fs', 'tp')
Inputs may be any that keep to these rules, and one draw needn't show every extreme that they name: `tokens`: activations whose features and rows have differing scales. `spatial_scale`: positive column scales.
All inputs are finite; a program needn't handle non-finite values.
Results may differ from a plain program's by a relative error of at most 0.019.
Values may be sent and summed in bfloat16 or wider, within the bound.
A program may use at most 128 MiB of HBM per device.

v0:
```python
import jax
import jax.numpy as jnp
from jax import lax
from jax.sharding import PartitionSpec as P

EPSILON = 1e-06


def normalize_rows(token_rows, gain_vector):
    values = token_rows.astype(jnp.float32)
    scaled = values * lax.rsqrt(jnp.mean(values * values, axis=-1, keepdims=True) + EPSILON)
    return (scaled * gain_vector).astype(jnp.bfloat16)


def shards(
    tokens,
    mixer_gain,
    w_content,
    w_spatial,
    content_scale,
    spatial_scale,
    spatial_gain,
    block_mixing,
    block_bias,
    w_project,
    project_scale,
    channel_gain,
    w_up,
    up_scale,
    w_down,
    down_scale,
):
    content_weight = w_content.astype(jnp.bfloat16)
    spatial_weight = w_spatial.astype(jnp.bfloat16)
    project_weight = w_project.astype(jnp.bfloat16)
    up_weight = w_up.astype(jnp.bfloat16)
    down_weight = w_down.astype(jnp.bfloat16)
    project_full, down_full = (
        lax.all_gather(project_scale, "fs", axis=0, tiled=True),
        lax.all_gather(down_scale, "fs", axis=0, tiled=True),
    )
    gathered_rows = lax.all_gather(tokens, "tp", axis=1, tiled=True)
    normed = normalize_rows(gathered_rows, mixer_gain)
    row_count = gathered_rows.shape[0]
    content_full, spatial_full, project_cols = (
        lax.all_gather(content_weight, "fs", axis=0, tiled=True),
        lax.all_gather(spatial_weight, "fs", axis=0, tiled=True),
        lax.all_gather(project_weight, "fs", axis=1, tiled=True),
    )
    content_linear = jnp.dot(normed, content_full, preferred_element_type=jnp.float32)
    spatial_linear = jnp.dot(normed, spatial_full, preferred_element_type=jnp.float32)
    content = jax.nn.gelu(content_linear * content_scale)
    spatial = jax.nn.gelu(spatial_linear * spatial_scale)
    square_sums = lax.psum(jnp.sum(spatial * spatial, axis=1), "tp")
    total_width = spatial.shape[1] * lax.axis_size("tp")
    spatial_norm = (
        spatial * lax.rsqrt(square_sums / total_width + EPSILON)[:, None] * spatial_gain
    ).astype(jnp.bfloat16)
    groups_here = block_mixing.shape[0]
    block_size = block_mixing.shape[1]
    group_width = spatial_norm.shape[1] // groups_here
    causal_mask = jnp.tril(jnp.ones((block_size, block_size), dtype=bool))
    mixing_weights = jnp.where(causal_mask[None, :, :], block_mixing, jnp.zeros_like(block_mixing))
    grouped = spatial_norm.reshape(row_count // block_size, block_size, groups_here, group_width)
    mixed_block = (
        jnp.einsum("gts,nsgc->ntgc", mixing_weights, grouped, preferred_element_type=jnp.float32)
        + block_bias.T[None, :, :, None]
    )
    gated = (content * mixed_block.reshape(row_count, spatial_norm.shape[1])).astype(jnp.bfloat16)
    mixer_terms = jnp.dot(gated, project_cols, preferred_element_type=jnp.float32) * project_full
    mixer_sum = lax.psum_scatter(
        mixer_terms.astype(jnp.bfloat16), "tp", scatter_dimension=1, tiled=True
    ).astype(jnp.float32)
    middle = (tokens.astype(jnp.float32) + mixer_sum).astype(jnp.bfloat16)
    middle_rows = lax.all_gather(middle, "tp", axis=1, tiled=True)
    channel_normed = normalize_rows(middle_rows, channel_gain)
    up_full, down_cols = (
        lax.all_gather(up_weight, "fs", axis=0, tiled=True),
        lax.all_gather(down_weight, "fs", axis=1, tiled=True),
    )
    up_linear = jnp.dot(channel_normed, up_full, preferred_element_type=jnp.float32)
    hidden = jnp.square(jax.nn.relu(up_linear * up_scale)).astype(jnp.bfloat16)
    channel_terms = jnp.dot(hidden, down_cols, preferred_element_type=jnp.float32) * down_full
    channel_sum = lax.psum_scatter(
        channel_terms.astype(jnp.bfloat16), "tp", scatter_dimension=1, tiled=True
    ).astype(jnp.float32)
    return (middle.astype(jnp.float32) + channel_sum).astype(jnp.bfloat16)


def solution(mesh):
    return jax.shard_map(
        shards,
        mesh=mesh,
        in_specs=(
            P("fs", "tp"),
            P(),
            P("fs", "tp"),
            P("fs", "tp"),
            P("tp"),
            P("tp"),
            P("tp"),
            P("tp", None, None),
            P("tp", None),
            P("tp", "fs"),
            P("fs"),
            P(),
            P("fs", "tp"),
            P("tp"),
            P("tp", "fs"),
            P("fs"),
        ),
        out_specs=P("fs", "tp"),
        check_vma=False,
    )
```

profile of v0, /device:TPU:0, one launch (start us, length us, event | category | flops | bytes accessed | tf_op | source)
XLA Modules:
  0.0 725.1 jit_solution(8672027433226947679)
XLA Ops:
  6.5 0.7 all-gather.10.cloned.1.call-update
  7.3 1.6 convert_element_type.64
  9.0 1.7 convert_element_type.63
  10.8 1.6 convert_element_type.67
  12.5 42.4 %all-gather = f32[16,1,128]{2,1,0:T(1,128)S(1)} all-gather(f32[1,1,128]{2,1,0:T(1,128)S(1)} %bitcast.30), channel_id=1, replica_groups=mesh['fs'=16,'tp'=2] {'fs'}, dimensions={0}, use_global_device_ids=true | all-gather | bytes 8704 | tf_op jit(solution)/shard_map/all_gather | solution.py:39
  55.0 1.8 fusion.1
  56.8 29.0 %all-gather.14.cloned.1.call-done = bf16[2048,512]{1,0:T(8,128)(2,1)} async-done(((bf16[128,512]{1,0:T(8,128)(2,1)}), bf16[2048,512]{1,0:T(8,128)(2,1)}) %all-gather.14.cloned.1.call-update) | async-done | bytes 2097168 | tf_op jit(solution)/shard_map/all_gather | solution.py:47
  85.8 3.4 multiply_reduce_fusion
  89.2 2.5 psum.7
  92.0 0.3 fusion.15
  92.6 55.2 %all-gather.12.cloned.1.call-done = bf16[2048,512]{1,0:T(8,128)(2,1)} async-done(((bf16[128,512]{1,0:T(8,128)(2,1)}), bf16[2048,512]{1,0:T(8,128)(2,1)}) %all-gather.12.cloned.1.call-update) | async-done | bytes 2097168 | tf_op jit(solution)/shard_map/all_gather | solution.py:46
  147.8 64.3 %all-gather.16.cloned.1.call-done = bf16[512,2048]{1,0:T(8,128)(2,1)} async-done(((bf16[512,128]{1,0:T(8,128)(2,1)}), bf16[512,2048]{1,0:T(8,128)(2,1)}) %all-gather.16.cloned.1.call-update) | async-done | bytes 2097168 | tf_op jit(solution)/shard_map/all_gather | solution.py:48
  212.1 5.5 multiply_convert_fusion.2
  217.7 7.2 reduce-scatter.3.cloned.1.call-done
  224.9 2.3 add_convert_fusion.1
  227.3 1.1 convert_element_type.74
  228.5 2.7 convert_element_type.76
  231.3 41.9 %all-gather.1 = f32[16,1,128]{2,1,0:T(1,128)S(1)} all-gather(f32[1,1,128]{2,1,0:T(1,128)S(1)} %bitcast.31), channel_id=1, replica_groups=mesh['fs'=16,'tp'=2] {'fs'}, dimensions={0}, use_global_device_ids=true | all-gather | bytes 8704 | tf_op jit(solution)/shard_map/all_gather | solution.py:40
  273.2 1.8 fusion.4
  275.0 158.5 %all-gather.20.cloned.1.call-done = bf16[2048,4096]{1,0:T(8,128)(2,1)} async-done(((bf16[128,4096]{1,0:T(8,128)(2,1)}), bf16[2048,4096]{1,0:T(8,128)(2,1)}) %all-gather.20.cloned.1.call-update) | async-done | bytes 16777232 | tf_op jit(solution)/shard_map/all_gather | solution.py:78
  433.5 250.0 %all-gather.22.cloned.1.call-done = bf16[4096,2048]{1,0:T(8,128)(2,1)} async-done(((bf16[4096,128]{1,0:T(8,128)(2,1)}), bf16[4096,2048]{1,0:T(8,128)(2,1)}) %all-gather.22.cloned.1.call-update) | async-done | bytes 16777232 | tf_op jit(solution)/shard_map/all_gather | solution.py:79
  683.5 25.4 %multiply_convert_fusion.1 = bf16[384,2048]{1,0:T(8,128)(2,1)} fusion(bf16[4096,2048]{1,0:T(8,128)(2,1)} %all-gather.22.cloned.1.call-done, bf16[2048,4096]{1,0:T(8,128)(2,1)} %all-gather.20.cloned.1.call-done, f32[4096]{0:T(1024)S(1)} %copy-done.9, bf16[384,2048]{1,0:T(8,128)(2,1)} %all-gather.18.cloned.1.call-done, f32[2048]{0:T(1024)S(1)} %bitcast.28, ...), kind=kOutput, calls=%fused_computation.12 | convolution fusion | flops 12895911936 | bytes 36734464 | tf_op jit(solution)/shard_map/dot_general | solution.py:83
  708.9 7.3 %reduce-scatter.5.cloned.1.call-done = bf16[384,1024]{1,0:T(8,128)(2,1)} async-done(((bf16[384,2048]{1,0:T(8,128)(2,1)}), bf16[384,1024]{1,0:T(8,128)(2,1)}) %reduce-scatter.5.cloned.1.call-update) | async-done | bytes 786448 | tf_op jit(solution)/shard_map/reduce_scatter | solution.py:84
  716.2 2.3 add_convert_fusion
  (54 shorter events, 1.1 us)
Async XLA Ops:
  6.5 5.9 copy-start.7
  6.5 79.3 %copy-start.10 = (f32[2048]{0:T(1024)S(1)}, f32[2048]{0:T(1024)}, u32[]{:S(2)}) copy-start(f32[2048]{0:T(1024)} %param.17) | copy-start | bytes 24580
  6.5 79.3 %copy-start.12 = (f32[512]{0:T(512)S(1)}, f32[512]{0:T(512)}, u32[]{:S(2)}) copy-start(f32[512]{0:T(512)} %param.21) | copy-start | bytes 6148
  6.5 48.4 %all-gather.10.cloned.1.call-start = ((), (), s32[]{:S(2)}) async-start(), calls=%async_computation.2 | async-start | bytes 2359296 | tf_op jit(solution)/shard_map/all_gather | solution.py:42
  7.3 78.5 %all-gather.14.cloned.1.call-start = ((), (), s32[]{:S(2)}) async-start(), calls=%async_computation.4 | async-start | bytes 2228224 | tf_op jit(solution)/shard_map/all_gather | solution.py:47
  9.0 138.8 %all-gather.12.cloned.1.call-start = ((), (), s32[]{:S(2)}) async-start(), calls=%async_computation.3 | async-start | bytes 2228224 | tf_op jit(solution)/shard_map/all_gather | solution.py:46
  10.7 201.4 %all-gather.16.cloned.1.call-start = ((), (), s32[]{:S(2)}) async-start(), calls=%async_computation.5 | async-start | bytes 2228224 | tf_op jit(solution)/shard_map/all_gather | solution.py:48
  12.4 212.5 %reduce-scatter.3.cloned.1.call-start = ((), (), s32[]{:S(2)}) async-start(), calls=%async_computation.6 | async-start | bytes 2359296 | tf_op jit(solution)/shard_map/reduce_scatter | solution.py:71
  56.8 34.9 %copy-start.5 = (f32[512]{0:T(512)S(1)}, f32[512]{0:T(512)}, u32[]{:S(2)}) copy-start(f32[512]{0:T(512)} %param.22) | copy-start | bytes 6148
  56.8 35.2 %copy-start.4 = (bf16[4,128,128]{2,1,0:T(8,128)(2,1)S(1)}, bf16[4,128,128]{2,1,0:T(8,128)(2,1)}, u32[]{:S(2)}) copy-start(bf16[4,128,128]{2,1,0:T(8,128)(2,1)} %param.23) | copy-start | bytes 393220
  56.8 35.2 %copy-start.6 = (f32[4,128]{1,0:T(4,128)S(1)}, f32[4,128]{1,0:T(4,128)}, u32[]{:S(2)}) copy-start(f32[4,128]{1,0:T(4,128)} %param.24) | copy-start | bytes 6148
  91.8 120.3 %copy-start.3 = (bf16[384,2048]{1,0:T(8,128)(2,1)S(1)}, bf16[384,2048]{1,0:T(8,128)(2,1)}, u32[]{:S(2)}) copy-start(bf16[384,2048]{1,0:T(8,128)(2,1)} %all-gather.10.cloned.1.call-done) | copy-start | bytes 4718596
  91.8 120.3 %copy-start.13 = (f32[512]{0:T(512)S(1)}, f32[512]{0:T(512)}, u32[]{:S(2)}) copy-start(f32[512]{0:T(512)} %param.20) | copy-start | bytes 6148
  217.6 7.3 %copy-start.1 = (bf16[384,1024]{1,0:T(8,128)(2,1)S(1)}, bf16[384,1024]{1,0:T(8,128)(2,1)}, u32[]{:S(2)}) copy-start(bf16[384,1024]{1,0:T(8,128)(2,1)} %param.16) | copy-start | bytes 2359300
  217.6 9.7 %copy-start.2 = (f32[128,4096]{1,0:T(8,128)S(1)}, f32[128,4096]{1,0:T(8,128)}, u32[]{:S(2)}) copy-start(f32[128,4096]{1,0:T(8,128)} %param.28) | copy-start | bytes 6291460
  217.6 55.5 %all-gather.18.cloned.1.call-start = ((), (), s32[]{:S(2)}) async-start(), calls=%async_computation.7 | async-start | bytes 2359296 | tf_op jit(solution)/shard_map/all_gather | solution.py:75
  227.3 206.2 %all-gather.20.cloned.1.call-start = ((), (), s32[]{:S(2)}) async-start(), calls=%async_computation.8 | async-start | bytes 17825792 | tf_op jit(solution)/shard_map/all_gather | solution.py:78
  228.5 2.8 copy-start.8
  228.5 455.1 %all-gather.22.cloned.1.call-start = ((), (), s32[]{:S(2)}) async-start(), calls=%async_computation.9 | async-start | bytes 17825792 | tf_op jit(solution)/shard_map/all_gather | solution.py:79
  231.2 452.3 %copy-start.9 = (f32[4096]{0:T(1024)S(1)}, f32[4096]{0:T(1024)}, u32[]{:S(2)}) copy-start(f32[4096]{0:T(1024)} %param.29) | copy-start | bytes 49156
  231.2 452.3 %copy-start.11 = (f32[2048]{0:T(1024)S(1)}, f32[2048]{0:T(1024)}, u32[]{:S(2)}) copy-start(f32[2048]{0:T(1024)} %param.27) | copy-start | bytes 24580
  231.3 485.0 %reduce-scatter.5.cloned.1.call-start = ((), (), s32[]{:S(2)}) async-start(), calls=%async_computation.10 | async-start | bytes 2359296 | tf_op jit(solution)/shard_map/reduce_scatter | solution.py:84
  708.9 7.3 %copy-start = (bf16[384,1024]{1,0:T(8,128)(2,1)S(1)}, bf16[384,1024]{1,0:T(8,128)(2,1)}, u32[]{:S(2)}) copy-start(bf16[384,1024]{1,0:T(8,128)(2,1)} %add_convert_fusion.1) | copy-start | bytes 2359300
Sparse Core Ops, SparseCore 0:
  8.9 12.5 all-gather.9
  24.2 61.5 all-gather.13
  88.6 59.1 all-gather.11
  150.3 61.7 all-gather.15
  217.8 7.1 reduce-scatter.2
  227.4 11.0 all-gather.17
  241.3 192.1 all-gather.19
  436.2 247.2 all-gather.21
  709.1 7.1 reduce-scatter.4
where the time goes:
time: 726 us; the launch traced here: 725 us
  waiting for transfers between devices  572 us (79%)
  blocking collectives  86.8 us (12%)
  matrix products  34.6 us (5%)
  other arithmetic  17.1 us (2%)
  between operations  13.3 us (2%)
    all_gather x1, waiting for transfers between devices, shards(): lax.all_gather(down_weight, 'fs', axis=1, tiled=True)  250 us
    all_gather x1, waiting for transfers between devices, shards(): lax.all_gather(up_weight, 'fs', axis=0, tiled=True)  159 us
    all_gather x1, waiting for transfers between devices, shards(): lax.all_gather(project_weight, 'fs', axis=1, tiled=True)  64.3 us
    all_gather x1, waiting for transfers between devices, shards(): lax.all_gather(content_weight, 'fs', axis=0, tiled=True)  55.2 us
    all_gather x1, blocking collectives, shards(): lax.all_gather(project_scale, 'fs', axis=0, tiled=True)  42.4 us
    all_gather x1, blocking collectives, shards(): lax.all_gather(down_scale, 'fs', axis=0, tiled=True)  41.9 us
    all_gather x1, waiting for transfers between devices, shards(): lax.all_gather(spatial_weight, 'fs', axis=0, tiled=True)  29 us
    dot_general x1, matrix products, shards(): jnp.dot(hidden, down_cols, preferred_element_type=jnp.float32) * down_full  25.4 us
  transfers between devices with their start and end apart: 9, of which 7 were waited for; matrix products, arithmetic and copies ran while one was open for 2% of the time, Pallas kernels for 0%

commit v1 on v0

--- a/solution.py
+++ b/solution.py
@@ -4,6 +4,12 @@
 from jax.sharding import PartitionSpec as P
 
 EPSILON = 1e-06
+
+
+def gathered_along(x, axis, dim):
+    shards = lax.all_gather(x, axis, axis=0, tiled=False)
+    result = jnp.concatenate(shards, axis=dim)
+    return result
 
 
 def normalize_rows(token_rows, gain_vector):
@@ -76,7 +82,7 @@
     channel_normed = normalize_rows(middle_rows, channel_gain)
     up_full, down_cols = (
         lax.all_gather(up_weight, "fs", axis=0, tiled=True),
-        lax.all_gather(down_weight, "fs", axis=1, tiled=True),
+        gathered_along(down_weight, "fs", 1),
     )
     up_linear = jnp.dot(channel_normed, up_full, preferred_element_type=jnp.float32)
     hidden = jnp.square(jax.nn.relu(up_linear * up_scale)).astype(jnp.bfloat16)

time: 726 us -> 662 us (0.912)
  waiting for transfers between devices: 572 us -> 493 us
  local copies, waits for them, and re-layouts: 0.48 us -> 21.6 us
    all_gather x1, waiting for transfers between devices: 250 us -> 159 us  [gathered_along(): shards = lax.all_gather(x, axis, axis=0, tiled=False)]
    reshape x0 -> x1, local copies, waits for them, and re-layouts: none -> 21.1 us  [gathered_along(): result = jnp.concatenate(shards, axis=dim)]
    all_gather x1, waiting for transfers between devices: 159 us -> 171 us  [shards(): lax.all_gather(up_weight, 'fs', axis=0, tiled=True)]
  transfers between devices with their start and end apart: 9 -> 9, of which waited for: 7 -> 7; matrix products, arithmetic and copies ran while one was open for 2% -> 6% of each run, Pallas kernels for 0% -> 0%
where the time goes in v1:
time: 662 us; the launch traced here: 661 us
  waiting for transfers between devices  493 us (74%)
  blocking collectives  86.8 us (13%)
  matrix products  28.6 us (4%)
  local copies, waits for them, and re-layouts  21.6 us (3%)
  other arithmetic  17.1 us (3%)
  between operations  13.3 us (2%)
    all_gather x1, waiting for transfers between devices, shards(): lax.all_gather(up_weight, 'fs', axis=0, tiled=True)  171 us
    all_gather x1, waiting for transfers between devices, gathered_along(): shards = lax.all_gather(x, axis, axis=0, tiled=False)  159 us
    all_gather x1, waiting for transfers between devices, shards(): lax.all_gather(project_weight, 'fs', axis=1, tiled=True)  64.3 us
    all_gather x1, waiting for transfers between devices, shards(): lax.all_gather(content_weight, 'fs', axis=0, tiled=True)  55.2 us
    all_gather x1, blocking collectives, shards(): lax.all_gather(project_scale, 'fs', axis=0, tiled=True)  42.6 us
    all_gather x1, blocking collectives, shards(): lax.all_gather(down_scale, 'fs', axis=0, tiled=True)  41.7 us
    all_gather x1, waiting for transfers between devices, shards(): lax.all_gather(spatial_weight, 'fs', axis=0, tiled=True)  28.9 us
    reshape x1, local copies, waits for them, and re-layouts, gathered_along(): result = jnp.concatenate(shards, axis=dim)  21.1 us
  transfers between devices with their start and end apart: 9, of which 7 were waited for; matrix products, arithmetic and copies ran while one was open for 6% of the time, Pallas kernels for 0%

profile of v1, /device:TPU:0, one launch (start us, length us, event | category | flops | bytes accessed | tf_op | source)
XLA Modules:
  0.0 661.1 jit_solution(17727143611421885555)
XLA Ops:
  6.5 0.7 all-gather.11.cloned.1.call-update
  7.3 1.6 convert_element_type.64
  9.0 1.6 convert_element_type.63
  10.7 1.6 convert_element_type.67
  12.4 42.6 %all-gather.1 = f32[16,1,128]{2,1,0:T(1,128)S(1)} all-gather(f32[1,1,128]{2,1,0:T(1,128)} %bitcast.36), channel_id=1, replica_groups=mesh['fs'=16,'tp'=2] {'fs'}, dimensions={0}, use_global_device_ids=true | all-gather | bytes 8704 | tf_op jit(solution)/shard_map/all_gather | solution.py:45
  55.1 1.8 fusion
  56.9 28.9 %all-gather.15.cloned.1.call-done = bf16[2048,512]{1,0:T(8,128)(2,1)} async-done(((bf16[128,512]{1,0:T(8,128)(2,1)}), bf16[2048,512]{1,0:T(8,128)(2,1)}) %all-gather.15.cloned.1.call-update) | async-done | bytes 2097168 | tf_op jit(solution)/shard_map/all_gather | solution.py:53
  85.8 3.4 multiply_reduce_fusion
  89.2 2.5 psum.7
  92.6 55.2 %all-gather.13.cloned.1.call-done = bf16[2048,512]{1,0:T(8,128)(2,1)} async-done(((bf16[128,512]{1,0:T(8,128)(2,1)}), bf16[2048,512]{1,0:T(8,128)(2,1)}) %all-gather.13.cloned.1.call-update) | async-done | bytes 2097168 | tf_op jit(solution)/shard_map/all_gather | solution.py:52
  147.8 64.3 %all-gather.17.cloned.1.call-done = bf16[512,2048]{1,0:T(8,128)(2,1)} async-done(((bf16[512,128]{1,0:T(8,128)(2,1)}), bf16[512,2048]{1,0:T(8,128)(2,1)}) %all-gather.17.cloned.1.call-update) | async-done | bytes 2097168 | tf_op jit(solution)/shard_map/all_gather | solution.py:54
  212.1 6.0 multiply_convert_fusion.2
  218.2 7.2 %reduce-scatter.3.cloned.1.call-done = bf16[384,1024]{1,0:T(8,128)(2,1)} async-done(((bf16[384,2048]{1,0:T(8,128)(2,1)}), bf16[384,1024]{1,0:T(8,128)(2,1)}) %reduce-scatter.3.cloned.1.call-update) | async-done | bytes 786448 | tf_op jit(solution)/shard_map/reduce_scatter | solution.py:77
  225.5 2.3 add_convert_fusion.1
  227.9 1.1 convert_element_type.76
  229.1 2.7 convert_element_type.74
  231.8 41.7 %all-gather.2 = f32[16,1,128]{2,1,0:T(1,128)S(1)} all-gather(f32[1,1,128]{2,1,0:T(1,128)S(1)} %bitcast.37), channel_id=1, replica_groups=mesh['fs'=16,'tp'=2] {'fs'}, dimensions={0}, use_global_device_ids=true | all-gather | bytes 8704 | tf_op jit(solution)/shard_map/all_gather | solution.py:46
  273.6 1.8 fusion.3
  275.4 158.7 %all-gather.23.cloned.1.call-done = bf16[65536,128]{1,0:T(8,128)(2,1)} async-done(((bf16[4096,128]{1,0:T(8,128)(2,1)}), bf16[65536,128]{1,0:T(8,128)(2,1)}) %all-gather.23.cloned.1.call-update) | async-done | bytes 16777232 | tf_op jit(solution)/shard_map/all_gather | solution.py:10
  434.1 21.1 %copy.26 = bf16[4096,16,128]{0,2,1:T(8,128)(2,1)} copy(bf16[4096,16,128]{2,0,1:T(8,128)(2,1)} %bitcast.30) | data formatting | bytes 33554432 | tf_op jit(solution)/shard_map/reshape | solution.py:11
  455.2 170.9 %all-gather.21.cloned.1.call-done = bf16[2048,4096]{1,0:T(8,128)(2,1)} async-done(((bf16[128,4096]{1,0:T(8,128)(2,1)}), bf16[2048,4096]{1,0:T(8,128)(2,1)}) %all-gather.21.cloned.1.call-update) | async-done | bytes 16777232 | tf_op jit(solution)/shard_map/all_gather | solution.py:84
  626.1 18.9 %multiply_convert_fusion.1 = bf16[384,2048]{1,0:T(8,128)(2,1)} fusion(bf16[4096,2048]{0,1:T(8,128)(2,1)} %bitcast.31, bf16[2048,4096]{1,0:T(8,128)(2,1)} %all-gather.21.cloned.1.call-done, f32[4096]{0:T(1024)S(1)} %copy-done.8, bf16[384,2048]{1,0:T(8,128)(2,1)S(1)} %copy-done.3, f32[2048]{0:T(1024)S(1)} %bitcast.34, f32[2048]{0:T(1024)S(1)} %copy-done.10, ...), kind=kOutput, calls=%fused_computation.11 | convolution fusion | flops 12895911936 | bytes 36734464 | tf_op jit(solution)/shard_map/dot_general | solution.py:89
  645.0 7.3 %reduce-scatter.5.cloned.1.call-done = bf16[384,1024]{1,0:T(8,128)(2,1)} async-done(((bf16[384,2048]{1,0:T(8,128)(2,1)}), bf16[384,1024]{1,0:T(8,128)(2,1)}) %reduce-scatter.5.cloned.1.call-update) | async-done | bytes 786448 | tf_op jit(solution)/shard_map/reduce_scatter | solution.py:90
  652.2 2.3 add_convert_fusion
  (53 shorter events, 1.5 us)
Async XLA Ops:
  6.5 79.3 %copy-start.9 = (f32[2048]{0:T(1024)S(1)}, f32[2048]{0:T(1024)}, u32[]{:S(2)}) copy-start(f32[2048]{0:T(1024)} %param.17) | copy-start | bytes 24580
  6.5 79.3 %copy-start.11 = (f32[512]{0:T(512)S(1)}, f32[512]{0:T(512)}, u32[]{:S(2)}) copy-start(f32[512]{0:T(512)} %param.21) | copy-start | bytes 6148
  6.5 48.5 %all-gather.11.cloned.1.call-start = ((), (), s32[]{:S(2)}) async-start(), calls=%async_computation.2 | async-start | bytes 2359296 | tf_op jit(solution)/shard_map/all_gather | solution.py:48
  7.3 78.5 %all-gather.15.cloned.1.call-start = ((), (), s32[]{:S(2)}) async-start(), calls=%async_computation.4 | async-start | bytes 2228224 | tf_op jit(solution)/shard_map/all_gather | solution.py:53
  9.0 138.8 %all-gather.13.cloned.1.call-start = ((), (), s32[]{:S(2)}) async-start(), calls=%async_computation.3 | async-start | bytes 2228224 | tf_op jit(solution)/shard_map/all_gather | solution.py:52
  10.7 201.4 %all-gather.17.cloned.1.call-start = ((), (), s32[]{:S(2)}) async-start(), calls=%async_computation.5 | async-start | bytes 2228224 | tf_op jit(solution)/shard_map/all_gather | solution.py:54
  12.4 213.1 %reduce-scatter.3.cloned.1.call-start = ((), (), s32[]{:S(2)}) async-start(), calls=%async_computation.6 | async-start | bytes 2359296 | tf_op jit(solution)/shard_map/reduce_scatter | solution.py:77
  56.9 34.8 %copy-start.5 = (f32[512]{0:T(512)S(1)}, f32[512]{0:T(512)}, u32[]{:S(2)}) copy-start(f32[512]{0:T(512)} %param.22) | copy-start | bytes 6148
  56.9 35.0 %copy-start.4 = (bf16[4,128,128]{2,1,0:T(8,128)(2,1)S(1)}, bf16[4,128,128]{2,1,0:T(8,128)(2,1)}, u32[]{:S(2)}) copy-start(bf16[4,128,128]{2,1,0:T(8,128)(2,1)} %param.23) | copy-start | bytes 393220
  56.9 35.0 %copy-start.6 = (f32[4,128]{1,0:T(4,128)S(1)}, f32[4,128]{1,0:T(4,128)}, u32[]{:S(2)}) copy-start(f32[4,128]{1,0:T(4,128)} %param.24) | copy-start | bytes 6148
  89.2 122.9 %copy-start.12 = (f32[512]{0:T(512)S(1)}, f32[512]{0:T(512)}, u32[]{:S(2)}) copy-start(f32[512]{0:T(512)} %param.20) | copy-start | bytes 6148
  212.1 13.4 %copy-start.1 = (bf16[384,1024]{1,0:T(8,128)(2,1)S(1)}, bf16[384,1024]{1,0:T(8,128)(2,1)}, u32[]{:S(2)}) copy-start(bf16[384,1024]{1,0:T(8,128)(2,1)} %param.16) | copy-start | bytes 2359300
  218.2 9.7 %copy-start.2 = (f32[4096,128]{1,0:T(8,128)S(1)}, f32[4096,128]{1,0:T(8,128)}, u32[]{:S(2)}) copy-start(f32[4096,128]{1,0:T(8,128)} %param.30) | copy-start | bytes 6291460
  218.2 55.4 %all-gather.19.cloned.1.call-start = ((), (), s32[]{:S(2)}) async-start(), calls=%async_computation.7 | async-start | bytes 2359296 | tf_op jit(solution)/shard_map/all_gather | solution.py:81
  227.8 206.2 %all-gather.23.cloned.1.call-start = ((), (), s32[]{:S(2)}) async-start(), calls=%async_computation.10 | async-start | bytes 17825792 | tf_op jit(solution)/shard_map/all_gather | solution.py:10
  229.0 2.8 copy-start.7
  229.0 397.0 %all-gather.21.cloned.1.call-start = ((), (), s32[]{:S(2)}) async-start(), calls=%async_computation.8 | async-start | bytes 17825792 | tf_op jit(solution)/shard_map/all_gather | solution.py:84
  231.8 420.5 %reduce-scatter.5.cloned.1.call-start = ((), (), s32[]{:S(2)}) async-start(), calls=%async_computation.9 | async-start | bytes 2359296 | tf_op jit(solution)/shard_map/reduce_scatter | solution.py:90
  434.1 192.0 %copy-start.3 = (bf16[384,2048]{1,0:T(8,128)(2,1)S(1)}, bf16[384,2048]{1,0:T(8,128)(2,1)}, u32[]{:S(2)}) copy-start(bf16[384,2048]{1,0:T(8,128)(2,1)} %all-gather.19.cloned.1.call-done) | copy-start | bytes 4718596
  434.1 192.0 %copy-start.8 = (f32[4096]{0:T(1024)S(1)}, f32[4096]{0:T(1024)}, u32[]{:S(2)}) copy-start(f32[4096]{0:T(1024)} %param.29) | copy-start | bytes 49156
  434.1 192.0 %copy-start.10 = (f32[2048]{0:T(1024)S(1)}, f32[2048]{0:T(1024)}, u32[]{:S(2)}) copy-start(f32[2048]{0:T(1024)} %param.27) | copy-start | bytes 24580
  626.1 26.2 %copy-start = (bf16[384,1024]{1,0:T(8,128)(2,1)S(1)}, bf16[384,1024]{1,0:T(8,128)(2,1)}, u32[]{:S(2)}) copy-start(bf16[384,1024]{1,0:T(8,128)(2,1)} %add_convert_fusion.1) | copy-start | bytes 2359300
Sparse Core Ops, SparseCore 0:
  8.9 12.5 all-gather.10
  24.2 61.5 all-gather.14
  88.6 59.1 all-gather.12
  150.3 61.7 all-gather.16
  218.3 7.1 reduce-scatter.2
  227.9 11.0 all-gather.18
  241.8 192.1 all-gather.22
  436.8 189.1 all-gather.20
  645.1 7.1 reduce-scatter.4
